TPU v7x, 32 devices: a whole 2x2x4 slice. The times are simulated.
32 devices in a mesh: fs: 8 (over z, x), tp: 4 (over y, core).
Axes of the slice: x: 2, y: 2, z: 4, core: 2. Of those that a mesh axis runs over, the one named last changes fastest.
Arguments:
- tokens: bfloat16 [4096, 2048], P('fs', 'tp'), may hold values from -16 to 16
- pre_mix_gain: bfloat16 [2048], P('tp'), may hold values from 0.099609375 to 1.8984375
- w_gate_in: bfloat16 [2048, 2048], P('fs', 'tp'), may hold values from -0.125 to 0.125
- w_input: bfloat16 [2048, 2048], P('fs', 'tp'), may hold values from -0.125 to 0.125
- mix_kernel: bfloat16 [4, 2048], P(None, 'tp'), may hold values from -3 to 3
- w_recur: bfloat16 [8, 256, 256], P('tp'), may hold values from -0.375 to 0.375
- w_inject: bfloat16 [8, 256, 256], P('tp'), may hold values from -0.375 to 0.375
- decay_param: float32 [2048], P('tp'), may hold values from 3 to 13
- w_mix_out: bfloat16 [2048, 2048], P('tp', 'fs'), may hold values from -0.125 to 0.125
- post_mix_gain: bfloat16 [2048], P('tp'), may hold values from 0.099609375 to 1.8984375
- pre_ffn_gain: bfloat16 [2048], P('tp'), may hold values from 0.099609375 to 1.8984375
- w_up_gate: bfloat16 [2048, 5632], P('fs', 'tp'), may hold values from -0.125 to 0.125
- w_up_value: bfloat16 [2048, 5632], P('fs', 'tp'), may hold values from -0.125 to 0.125
- gate_kernel: bfloat16 [3, 5632], P(None, 'tp'), may hold values from -3 to 3
- value_kernel: bfloat16 [3, 5632], P(None, 'tp'), may hold values from -3 to 3
- w_down: bfloat16 [5632, 2048], P('tp', 'fs'), may hold values from -0.078125 to 0.078125
- post_ffn_gain: bfloat16 [2048], P('tp'), may hold values from 0.099609375 to 1.8984375
Outputs:
- layer_out: bfloat16 [4096, 2048], P('fs', 'tp')
All inputs are finite; a program needn't handle non-finite values.
Results may differ from a plain program's by a relative error of at most 0.015.
Values may be sent and summed in bfloat16 or wider, within the bound.
A program may use at most 64 MiB of HBM per device.

v0:
```python
import jax
import jax.numpy as jnp
from jax import lax
from jax.sharding import PartitionSpec as P

D = 2048
norm_eps = 1e-06
gate_power = 8.0


def row_normed(values, row_gain):
    widened = values.astype(jnp.float32)
    squares = lax.psum(jnp.sum(widened * widened, axis=1), "tp")
    factor = lax.rsqrt(squares / D + norm_eps)
    return widened * factor[:, None] * row_gain.astype(jnp.float32)[None, :]


def gathered_rows(values, row_gain):
    return lax.all_gather(
        row_normed(values, row_gain).astype(jnp.bfloat16), "tp", axis=1, tiled=True
    )


def summed_terms(partial_value):
    return lax.psum_scatter(
        partial_value.astype(jnp.bfloat16), "tp", scatter_dimension=1, tiled=True
    ).astype(jnp.float32)


def causal_conv(values, kernel):
    length = values.shape[0]
    widths = kernel.shape[0]
    padded = jnp.pad(values.astype(jnp.float32), ((widths - 1, 0), (0, 0)))
    weights = kernel.astype(jnp.float32)
    result = padded[0:length] * weights[0]
    for offset in range(1, widths):
        result = result + padded[offset : offset + length] * weights[offset]
    return result


def pair_folder(inputs, pieces):
    return (
        jnp.dot(inputs, pieces[0], preferred_element_type=jnp.float32),
        jnp.dot(inputs, pieces[1], preferred_element_type=jnp.float32),
    )


def linear_combine(earlier, latter):
    return (earlier[0] * latter[0], latter[0] * earlier[1] + latter[1])


def shards(
    tokens,
    pre_mix_gain,
    w_gate_in,
    w_input,
    mix_kernel,
    w_recur,
    w_inject,
    decay_param,
    w_mix_out,
    post_mix_gain,
    pre_ffn_gain,
    w_up_gate,
    w_up_value,
    gate_kernel,
    value_kernel,
    w_down,
    post_ffn_gain,
):
    normed_in = gathered_rows(tokens, pre_mix_gain)
    length = normed_in.shape[0]
    gate_sum, input_sum = pair_folder(
        normed_in,
        (
            lax.all_gather(w_gate_in, "fs", axis=0, tiled=True),
            lax.all_gather(w_input, "fs", axis=0, tiled=True),
        ),
    )
    gate_rows = gate_sum.astype(jnp.bfloat16)
    input_rows = input_sum.astype(jnp.bfloat16)
    smoothed = causal_conv(input_rows, mix_kernel).astype(jnp.bfloat16)
    by_head = smoothed.reshape(length, w_recur.shape[0], w_recur.shape[1])
    recur_gate = jax.nn.sigmoid(
        jnp.einsum("thi,hij->thj", by_head, w_recur, preferred_element_type=jnp.float32)
    ).reshape(length, -1)
    inject_gate = jax.nn.sigmoid(
        jnp.einsum("thi,hij->thj", by_head, w_inject, preferred_element_type=jnp.float32)
    ).reshape(length, -1)
    log_retain = -gate_power * recur_gate * jax.nn.softplus(-decay_param)[None, :]
    retain = jnp.exp(log_retain)
    driven = jnp.sqrt(-jnp.expm1(2.0 * log_retain)) * inject_gate * smoothed.astype(jnp.float32)
    _, states = lax.associative_scan(linear_combine, (retain, driven), axis=0)
    hidden = (jax.nn.gelu(gate_rows.astype(jnp.float32), approximate=True) * states).astype(
        jnp.bfloat16
    )
    mixer_terms = jnp.dot(
        hidden,
        lax.all_gather(w_mix_out, "fs", axis=1, tiled=True),
        preferred_element_type=jnp.float32,
    )
    middle = (
        tokens.astype(jnp.float32) + row_normed(summed_terms(mixer_terms), post_mix_gain)
    ).astype(jnp.bfloat16)
    normed_mid = gathered_rows(middle, pre_ffn_gain)
    up_gate, up_value = pair_folder(
        normed_mid,
        (
            lax.all_gather(w_up_gate, "fs", axis=0, tiled=True),
            lax.all_gather(w_up_value, "fs", axis=0, tiled=True),
        ),
    )
    conv_gate_out = causal_conv(up_gate.astype(jnp.bfloat16), gate_kernel)
    conv_value_out = causal_conv(up_value.astype(jnp.bfloat16), value_kernel)
    activated = (jax.nn.gelu(conv_gate_out, approximate=True) * conv_value_out).astype(jnp.bfloat16)
    ffn_terms = jnp.dot(
        activated,
        lax.all_gather(w_down, "fs", axis=1, tiled=True),
        preferred_element_type=jnp.float32,
    )
    return (middle.astype(jnp.float32) + row_normed(summed_terms(ffn_terms), post_ffn_gain)).astype(
        jnp.bfloat16
    )


def solution(mesh):
    return jax.shard_map(
        shards,
        mesh=mesh,
        in_specs=(
            P("fs", "tp"),
            P("tp"),
            P("fs", "tp"),
            P("fs", "tp"),
            P(None, "tp"),
            P("tp", None, None),
            P("tp", None, None),
            P("tp"),
            P("tp", "fs"),
            P("tp"),
            P("tp"),
            P("fs", "tp"),
            P("fs", "tp"),
            P(None, "tp"),
            P(None, "tp"),
            P("tp", "fs"),
            P("tp"),
        ),
        out_specs=P("fs", "tp"),
        check_vma=False,
    )
```

profile of v0, /device:TPU:0, one launch (start us, length us, event | category | flops | bytes accessed | tf_op | source)
XLA Modules:
  0.0 595.2 jit_solution(16134172578060432192)
XLA Ops:
  7.8 8.4 %psum.28 = f32[512]{0:T(512)S(1)} all-reduce(f32[512]{0:T(512)S(1)} %fusion.33), channel_id=1, replica_groups=mesh['fs'=8,'tp'=4] {'tp'}, use_global_device_ids=true, to_apply=%region_1.0 | all-reduce | flops 512 | bytes 4096 | tf_op jit(solution)/shard_map/psum | solution.py:13
  16.9 2.0 fusion.35
  21.1 20.8 %all-gather.9.cloned.1.call-done = bf16[512,2048]{1,0:T(8,128)(2,1)} async-done(((bf16[512,512]{1,0:T(8,128)(2,1)}), bf16[512,2048]{1,0:T(8,128)(2,1)}) %all-gather.9.cloned.1.call-update) | async-done | bytes 2097168 | tf_op jit(solution)/shard_map/all_gather | solution.py:19
  42.0 51.2 %all-gather.13.cloned.1.call-done = bf16[2048,512]{1,0:T(8,128)(2,1)} async-done(((bf16[256,512]{1,0:T(8,128)(2,1)}), bf16[2048,512]{1,0:T(8,128)(2,1)}) %all-gather.13.cloned.1.call-update) | async-done | bytes 2097168 | tf_op jit(solution)/shard_map/all_gather | solution.py:77
  93.2 3.5 fusion.28
  97.7 1.3 copy.26
  99.5 1.4 copy.27
  100.9 2.8 multiply_exponential_fusion
  103.7 2.1 slice.271
  105.8 2.1 slice.272
  107.8 2.1 slice.270
  109.9 2.1 slice.274
  112.0 1.7 fusion.78
  113.7 1.4 slice.277
  115.1 1.4 slice.278
  116.5 1.4 slice.276
  117.8 1.4 slice.280
  119.2 2.0 fusion.79
  122.6 1.6 slice.282
  124.2 1.6 slice.286
  125.8 1.8 fusion.80
  128.8 1.5 slice.288
  130.3 1.5 slice.292
  131.9 1.6 fusion.81
  133.4 1.4 slice.295
  134.9 1.4 slice.296
  136.3 1.4 slice.294
  137.8 1.4 slice.298
  139.2 1.4 fusion.82
  140.7 1.4 slice.301
  142.0 1.4 slice.302
  143.4 1.4 slice.300
  144.8 1.4 slice.304
  146.1 1.4 fusion.83
  148.7 1.3 slice.306
  150.0 1.3 slice.310
  151.3 1.4 fusion.85
  152.7 1.3 slice.313
  155.3 1.3 slice.312
  157.9 1.3 slice.305
  161.2 1.4 slice.324
  162.5 1.3 slice.354
  163.8 1.4 slice.293
  165.3 1.5 slice.326
  168.0 1.5 slice.287
  173.3 1.4 slice.275
  174.7 1.4 slice.332
  184.8 2.8 pad.84
  188.1 5.7 all-gather.15.cloned.1.call-done
  193.8 7.2 %convolution_convert_fusion.2 = bf16[512,2048]{1,0:T(8,128)(2,1)} fusion(bf16[512,2048]{1,0:T(8,128)(2,1)} %all-gather.15.cloned.1.call-done, bf16[512,2048]{1,0:T(8,128)(2,1)} %all-gather.9.cloned.1.call-done, bf16[2048,512]{1,0:T(8,128)(2,1)} %all-gather.11.cloned.1.call-done, f32[512,512]{1,0:T(8,128)S(1)} %pad.83, f32[512,512]{1,0:T(8,128)} %pad.84), kind=kOutput, calls=%fused_computation.5 | convolution fusion | flops 2151940096 | bytes 10485760 | tf_op jit(solution)/shard_map/dot_general | solution.py:97
  201.7 28.8 %reduce-scatter.3.cloned.1.call-done = bf16[512,512]{1,0:T(8,128)(2,1)} async-done(((bf16[512,2048]{1,0:T(8,128)(2,1)}), bf16[512,512]{1,0:T(8,128)(2,1)}) %reduce-scatter.3.cloned.1.call-update) | async-done | bytes 524304 | tf_op jit(solution)/shard_map/reduce_scatter | solution.py:25
  231.7 5.8 psum.29
  237.5 1.5 fusion.37
  239.0 5.7 psum.30
  247.3 77.5 %all-gather.21.cloned.1.call-done = bf16[2048,1408]{1,0:T(8,128)(2,1)} async-done(((bf16[256,1408]{1,0:T(8,128)(2,1)}), bf16[2048,1408]{1,0:T(8,128)(2,1)}) %all-gather.21.cloned.1.call-update) | async-done | bytes 5767184 | tf_op jit(solution)/shard_map/all_gather | solution.py:110
  324.9 22.3 %all-gather.17.cloned.1.call-done = bf16[512,2048]{1,0:T(8,128)(2,1)} async-done(((bf16[512,512]{1,0:T(8,128)(2,1)}), bf16[512,2048]{1,0:T(8,128)(2,1)}) %all-gather.17.cloned.1.call-update) | async-done | bytes 2097168 | tf_op jit(solution)/shard_map/all_gather | solution.py:19
  347.2 8.4 %fusion = f32[512,1408]{1,0:T(8,128)} fusion(bf16[512,2048]{1,0:T(8,128)(2,1)} %all-gather.17.cloned.1.call-done, bf16[2048,1408]{1,0:T(8,128)(2,1)} %all-gather.21.cloned.1.call-done), kind=kOutput, calls=%fused_computation.2 | convolution fusion | flops 2954231808 | bytes 10747904 | tf_op jit(solution)/shard_map/dot_general | solution.py:44
  355.6 86.1 %all-gather.19.cloned.1.call-done = bf16[2048,1408]{1,0:T(8,128)(2,1)} async-done(((bf16[256,1408]{1,0:T(8,128)(2,1)}), bf16[2048,1408]{1,0:T(8,128)(2,1)}) %all-gather.19.cloned.1.call-update) | async-done | bytes 5767184 | tf_op jit(solution)/shard_map/all_gather | solution.py:109
  441.8 7.6 %fusion.1 = f32[512,1408]{1,0:T(8,128)} fusion(bf16[512,2048]{1,0:T(8,128)(2,1)S(1)} %copy-done.26, bf16[2048,1408]{1,0:T(8,128)(2,1)} %all-gather.19.cloned.1.call-done), kind=kOutput, calls=%fused_computation.4 | convolution fusion | flops 2954231808 | bytes 10747904 | tf_op jit(solution)/shard_map/dot_general | solution.py:43
  449.4 85.8 %all-gather.23.cloned.1.call-done = bf16[1408,2048]{1,0:T(8,128)(2,1)} async-done(((bf16[1408,256]{1,0:T(8,128)(2,1)}), bf16[1408,2048]{1,0:T(8,128)(2,1)}) %all-gather.23.cloned.1.call-update) | async-done | bytes 5767184 | tf_op jit(solution)/shard_map/all_gather | solution.py:118
  535.2 14.5 %convolution_convert_fusion.3 = bf16[512,2048]{1,0:T(8,128)(2,1)} fusion(bf16[1408,2048]{1,0:T(8,128)(2,1)} %all-gather.23.cloned.1.call-done, f32[512,1408]{1,0:T(8,128)} %fusion, f32[512,1408]{1,0:T(8,128)} %fusion.1, f32[1408]{0:T(1024)S(1)} %get-tuple-element.9, f32[1408]{0:T(1024)S(1)} %get-tuple-element.10, f32[1408]{0:T(1024)S(1)} %get-tuple-element.8, ...), kind=kOutput, calls=%fused_computation.6 | convolution fusion | flops 2968256512 | bytes 13665280 | tf_op jit(solution)/shard_map/dot_general | solution.py:116
  549.7 29.5 %reduce-scatter.5.cloned.1.call-done = bf16[512,512]{1,0:T(8,128)(2,1)} async-done(((bf16[512,2048]{1,0:T(8,128)(2,1)}), bf16[512,512]{1,0:T(8,128)(2,1)}) %reduce-scatter.5.cloned.1.call-update) | async-done | bytes 524304 | tf_op jit(solution)/shard_map/reduce_scatter | solution.py:25
  580.5 5.8 psum.31
  586.2 2.1 fusion.40
  (159 shorter events, 33.4 us)
Async XLA Ops:
  6.5 90.6 %copy-start = (bf16[2,256,256]{2,1,0:T(8,128)(2,1)S(1)}, bf16[2,256,256]{2,1,0:T(8,128)(2,1)}, u32[]{:S(2)}) copy-start(bf16[2,256,256]{2,1,0:T(8,128)(2,1)} %param.22) | copy-start | bytes 786436
  6.5 14.5 %copy-start.12 = (bf16[4,512]{1,0:T(4,128)(2,1)S(1)}, bf16[4,512]{1,0:T(4,128)(2,1)}, u32[]{:S(2)}) copy-start(bf16[4,512]{1,0:T(4,128)(2,1)} %param.21) | copy-start | bytes 12292
  6.5 14.5 %copy-start.22 = (f32[512]{0:T(512)S(1)}, f32[512]{0:T(512)}, u32[]{:S(2)}) copy-start(f32[512]{0:T(512)} %param.24) | copy-start | bytes 6148
  6.5 35.4 %all-gather.9.cloned.1.call-start = ((), (), s32[]{:S(2)}) async-start(), calls=%async_computation.2 | async-start | bytes 2621440 | tf_op jit(solution)/shard_map/all_gather | solution.py:19
  18.9 74.3 %all-gather.13.cloned.1.call-start = ((), (), s32[]{:S(2)}) async-start(), calls=%async_computation.4 | async-start | bytes 2359296 | tf_op jit(solution)/shard_map/all_gather | solution.py:77
  19.7 168.4 %all-gather.11.cloned.1.call-start = ((), (), s32[]{:S(2)}) async-start(), calls=%async_computation.3 | async-start | bytes 2359296 | tf_op jit(solution)/shard_map/all_gather | solution.py:76
  20.4 173.4 %all-gather.15.cloned.1.call-start = ((), (), s32[]{:S(2)}) async-start(), calls=%async_computation.5 | async-start | bytes 2359296 | tf_op jit(solution)/shard_map/all_gather | solution.py:99
  21.0 209.5 %reduce-scatter.3.cloned.1.call-start = ((), (), s32[]{:S(2)}) async-start(), calls=%async_computation.6 | async-start | bytes 2621440 | tf_op jit(solution)/shard_map/reduce_scatter | solution.py:25
  97.2 1.8 copy-start.27
  173.2 5.2 copy-start.11
  173.2 5.2 copy-start.13
  173.2 5.2 copy-start.14
  173.2 5.2 copy-start.17
  173.2 5.2 copy-start.8
  173.2 6.0 %copy-start.9 = (f32[3,512]{1,0:T(4,128)S(1)}, f32[3,512]{1,0:T(4,128)}, u32[]{:S(2)}) copy-start(f32[3,512]{1,0:T(4,128)} %slice.305) | copy-start | bytes 18436
  173.2 6.0 %copy-start.10 = (f32[3,512]{1,0:T(4,128)S(1)}, f32[3,512]{1,0:T(4,128)}, u32[]{:S(2)}) copy-start(f32[3,512]{1,0:T(4,128)} %slice.322) | copy-start | bytes 18436
  173.3 6.1 %copy-start.21 = (f32[1,512]{1,0:T(1,128)S(1)}, f32[1,512]{1,0:T(1,128)}, u32[]{:S(2)}) copy-start(f32[1,512]{1,0:T(1,128)} %slice.355) | copy-start | bytes 6148
  173.3 6.1 %copy-start.7 = (f32[7,512]{1,0:T(8,128)S(1)}, f32[7,512]{1,0:T(8,128)}, u32[]{:S(2)}) copy-start(f32[7,512]{1,0:T(8,128)} %slice.324) | copy-start | bytes 43012
  173.3 6.1 %copy-start.20 = (f32[1,512]{1,0:T(1,128)S(1)}, f32[1,512]{1,0:T(1,128)}, u32[]{:S(2)}) copy-start(f32[1,512]{1,0:T(1,128)} %slice.354) | copy-start | bytes 6148
  173.3 6.2 %copy-start.6 = (f32[15,512]{1,0:T(8,128)S(1)}, f32[15,512]{1,0:T(8,128)}, u32[]{:S(2)}) copy-start(f32[15,512]{1,0:T(8,128)} %slice.293) | copy-start | bytes 92164
  173.3 7.7 %copy-start.5 = (f32[31,512]{1,0:T(8,128)S(1)}, f32[31,512]{1,0:T(8,128)}, u32[]{:S(2)}) copy-start(f32[31,512]{1,0:T(8,128)} %slice.287) | copy-start | bytes 190468
  177.8 6.6 %copy-start.3 = (f32[127,512]{1,0:T(8,128)S(1)}, f32[127,512]{1,0:T(8,128)}, u32[]{:S(2)}) copy-start(f32[127,512]{1,0:T(8,128)} %slice.275) | copy-start | bytes 780292
  177.8 6.6 %copy-start.4 = (f32[127,512]{1,0:T(8,128)S(1)}, f32[127,512]{1,0:T(8,128)}, u32[]{:S(2)}) copy-start(f32[127,512]{1,0:T(8,128)} %slice.332) | copy-start | bytes 780292
  179.5 5.1 copy-start.19
  184.7 3.2 copy-start.18
  188.1 13.6 %copy-start.23 = (bf16[512]{0:T(512)(128)(2,1)S(1)}, bf16[512]{0:T(512)(128)(2,1)}, u32[]{:S(2)}) copy-start(bf16[512]{0:T(512)(128)(2,1)} %param.26) | copy-start | bytes 3076
  188.1 13.6 %copy-start.24 = (bf16[512]{0:T(512)(128)(2,1)S(1)}, bf16[512]{0:T(512)(128)(2,1)}, u32[]{:S(2)}) copy-start(bf16[512]{0:T(512)(128)(2,1)} %param.27) | copy-start | bytes 3076
  201.0 36.5 %copy-start.2 = (bf16[512,512]{1,0:T(8,128)(2,1)S(1)}, bf16[512,512]{1,0:T(8,128)(2,1)}, u32[]{:S(2)}) copy-start(bf16[512,512]{1,0:T(8,128)(2,1)} %param.17) | copy-start | bytes 1572868
  201.0 46.2 %copy-start.15 = (bf16[3,1408]{1,0:T(4,128)(2,1)S(1)}, bf16[3,1408]{1,0:T(4,128)(2,1)}, u32[]{:S(2)}) copy-start(bf16[3,1408]{1,0:T(4,128)(2,1)} %param.30) | copy-start | bytes 25348
  201.0 46.2 %copy-start.16 = (bf16[3,1408]{1,0:T(4,128)(2,1)S(1)}, bf16[3,1408]{1,0:T(4,128)(2,1)}, u32[]{:S(2)}) copy-start(bf16[3,1408]{1,0:T(4,128)(2,1)} %param.31) | copy-start | bytes 25348
  201.0 123.9 %all-gather.21.cloned.1.call-start = ((), (), s32[]{:S(2)}) async-start(), calls=%async_computation.9 | async-start | bytes 6488064 | tf_op jit(solution)/shard_map/all_gather | solution.py:110
  201.6 145.6 %all-gather.17.cloned.1.call-start = ((), (), s32[]{:S(2)}) async-start(), calls=%async_computation.7 | async-start | bytes 2621440 | tf_op jit(solution)/shard_map/all_gather | solution.py:19
  245.7 196.1 %all-gather.19.cloned.1.call-start = ((), (), s32[]{:S(2)}) async-start(), calls=%async_computation.8 | async-start | bytes 6488064 | tf_op jit(solution)/shard_map/all_gather | solution.py:109
  246.4 288.7 %all-gather.23.cloned.1.call-start = ((), (), s32[]{:S(2)}) async-start(), calls=%async_computation.10 | async-start | bytes 6488064 | tf_op jit(solution)/shard_map/all_gather | solution.py:118
  247.1 332.1 %reduce-scatter.5.cloned.1.call-start = ((), (), s32[]{:S(2)}) async-start(), calls=%async_computation.11 | async-start | bytes 2621440 | tf_op jit(solution)/shard_map/reduce_scatter | solution.py:25
  347.2 94.5 %copy-start.26 = (bf16[512,2048]{1,0:T(8,128)(2,1)S(1)}, bf16[512,2048]{1,0:T(8,128)(2,1)}, u32[]{:S(2)}) copy-start(bf16[512,2048]{1,0:T(8,128)(2,1)} %all-gather.17.cloned.1.call-done) | copy-start | bytes 6291460
  535.1 14.6 %copy-start.25 = (bf16[512]{0:T(512)(128)(2,1)S(1)}, bf16[512]{0:T(512)(128)(2,1)}, u32[]{:S(2)}) copy-start(bf16[512]{0:T(512)(128)(2,1)} %param.33) | copy-start | bytes 3076
  535.2 53.2 %copy-start.1 = (bf16[2,256,256]{2,1,0:T(8,128)(2,1)S(1)}, bf16[2,256,256]{2,1,0:T(8,128)(2,1)}, u32[]{:S(2)}) copy-start(bf16[2,256,256]{2,1,0:T(8,128)(2,1)} %param.22) | copy-start | bytes 786436
Sparse Core Ops, SparseCore 0:
  19.1 22.8 all-gather.8
  44.1 49.0 all-gather.12
  95.3 47.6 all-gather.10
  144.9 48.8 all-gather.14
  201.1 29.3 reduce-scatter.2
  232.5 92.2 all-gather.20
  326.4 20.7 all-gather.16
  349.4 92.2 all-gather.18
  443.8 91.3 all-gather.22
  549.8 29.3 reduce-scatter.4
where the time goes:
time: 597 us; the launch traced here: 595 us
  waiting for transfers between devices  412 us (69%)
  local copies, waits for them, and re-layouts  69.6 us (12%)
  matrix products  42.1 us (7%)
  other arithmetic  31.5 us (5%)
  blocking collectives  25.6 us (4%)
  between operations  14.2 us (2%)
    all_gather x1, waiting for transfers between devices, shards(): lax.all_gather(w_up_gate, 'fs', axis=0, tiled=True)  86.1 us
    all_gather x1, waiting for transfers between devices, shards(): lax.all_gather(w_down, 'fs', axis=1, tiled=True)  85.8 us
    all_gather x1, waiting for transfers between devices, shards(): lax.all_gather(w_up_value, 'fs', axis=0, tiled=True)  77.5 us
    slice x53, local copies, waits for them, and re-layouts, shards(): _, states = lax.associative_scan(linear_combine, (retain, driven), axis=0)  63.3 us
    reduce_scatter x2, waiting for transfers between devices, summed_terms(): lax.psum_scatter(partial_value.astype(jnp.bfloat16), 'tp', scatter_dimens...  58.3 us
    all_gather x1, waiting for transfers between devices, shards(): lax.all_gather(w_input, 'fs', axis=0, tiled=True)  51.2 us
    all_gather x2, waiting for transfers between devices, gathered_rows(): lax.all_gather(row_normed(values, row_gain).astype(jnp.bfloat16), 'tp', a...  43.2 us
    psum x4, blocking collectives, row_normed(): squares = lax.psum(jnp.sum(widened * widened, axis=1), 'tp')  25.6 us
  transfers between devices with their start and end apart: 10, of which 9 were waited for; matrix products, arithmetic and copies ran while one was open for 19% of the time, Pallas kernels for 0%

commit v1 on v0

--- a/solution.py
+++ b/solution.py
@@ -1,3 +1,4 @@
+import functools
 import jax
 import jax.numpy as jnp
 from jax import lax
@@ -8,6 +9,15 @@
 gate_power = 8.0
 
 
+def step_on_points(message, bus_axis, k_dim):
+    shaped = lax.all_to_all(jnp.stack([message] * lax.axis_size(bus_axis)), bus_axis, 0, 0)
+    tile_out = jnp.concatenate(shaped, axis=k_dim)
+    return tile_out
+
+
+replace_task = functools.partial(step_on_points, bus_axis="tp", k_dim=1)
+
+
 def row_normed(values, row_gain):
     widened = values.astype(jnp.float32)
     squares = lax.psum(jnp.sum(widened * widened, axis=1), "tp")
@@ -16,9 +26,7 @@
 
 
 def gathered_rows(values, row_gain):
-    return lax.all_gather(
-        row_normed(values, row_gain).astype(jnp.bfloat16), "tp", axis=1, tiled=True
-    )
+    return replace_task(row_normed(values, row_gain).astype(jnp.bfloat16))
 
 
 def summed_terms(partial_value):

time: 597 us -> 542 us (0.908)
  waiting for transfers between devices: 412 us -> 348 us
  starting transfers between devices: 0.54 us -> 7.62 us
    all_to_all x0 -> x2, waiting for transfers between devices: none -> 50.2 us  [step_on_points(): lax.all_to_all(jnp.stack([message] * lax.axis_size(bus_axis)), bus_axis,...]
    all_gather x2 -> x0, waiting for transfers between devices: 43.2 us -> none  [gathered_rows(): lax.all_gather(row_normed(values, row_gain).astype(jnp.bfloat16), 'tp', a...]
    all_gather x1, waiting for transfers between devices: 51.2 us -> 10.6 us  [shards(): lax.all_gather(w_input, 'fs', axis=0, tiled=True)]
    all_gather x1, waiting for transfers between devices: 77.5 us -> 48.9 us  [shards(): lax.all_gather(w_up_value, 'fs', axis=0, tiled=True)]
    all_to_all x0 -> x2, starting transfers between devices: none -> 7.34 us  [step_on_points(): lax.all_to_all(jnp.stack([message] * lax.axis_size(bus_axis)), bus_axis,...]
    all_gather x1, waiting for transfers between devices: 0.02 us -> 6.13 us  [shards(): lax.all_gather(w_gate_in, 'fs', axis=0, tiled=True)]
  transfers between devices with their start and end apart: 10 -> 10, of which waited for: 9 -> 9; matrix products, arithmetic and copies ran while one was open for 19% -> 22% of each run, Pallas kernels for 0% -> 0%
where the time goes in v1:
time: 542 us; the launch traced here: 539 us
  waiting for transfers between devices  348 us (64%)
  local copies, waits for them, and re-layouts  73 us (13%)
  matrix products  41 us (8%)
  other arithmetic  29.9 us (6%)
  blocking collectives  25.8 us (5%)
  between operations  14.2 us (3%)
  starting transfers between devices  7.62 us (1%)
    all_gather x1, waiting for transfers between devices, shards(): lax.all_gather(w_down, 'fs', axis=1, tiled=True)  85.6 us
    all_gather x1, waiting for transfers between devices, shards(): lax.all_gather(w_up_gate, 'fs', axis=0, tiled=True)  84.9 us
    slice x53, local copies, waits for them, and re-layouts, shards(): _, states = lax.associative_scan(linear_combine, (retain, driven), axis=0)  63.4 us
    reduce_scatter x2, waiting for transfers between devices, summed_terms(): lax.psum_scatter(partial_value.astype(jnp.bfloat16), 'tp', scatter_dimens...  57.4 us
    all_to_all x2, waiting for transfers between devices, step_on_points(): lax.all_to_all(jnp.stack([message] * lax.axis_size(bus_axis)), bus_axis,...  50.2 us
    all_gather x1, waiting for transfers between devices, shards(): lax.all_gather(w_up_value, 'fs', axis=0, tiled=True)  48.9 us
    psum x4, blocking collectives, row_normed(): squares = lax.psum(jnp.sum(widened * widened, axis=1), 'tp')  25.8 us
    dot_general x1, matrix products, shards(): jnp.dot(activated, lax.all_gather(w_down, 'fs', axis=1, tiled=True), pref...  14.7 us
  transfers between devices with their start and end apart: 10, of which 9 were waited for; matrix products, arithmetic and copies ran while one was open for 22% of the time, Pallas kernels for 0%

profile of v1, /device:TPU:0, one launch (start us, length us, event | category | flops | bytes accessed | tf_op | source)
XLA Modules:
  0.0 539.2 jit_solution(3861532676276726477)
XLA Ops:
  9.9 8.4 %psum.28 = f32[512]{0:T(512)S(1)} all-reduce(f32[512]{0:T(512)S(1)} %fusion.33), channel_id=1, replica_groups=mesh['fs'=8,'tp'=4] {'tp'}, use_global_device_ids=true, to_apply=%region_1.0 | all-reduce | flops 512 | bytes 4096 | tf_op jit(solution)/shard_map/psum | solution.py:23
  19.8 1.5 stack.4
  21.3 3.7 all-to-all-start
  25.9 24.8 %all-to-all-done = bf16[4,512,512]{1,2,0:T(8,128)(2,1)S(1)} async-done(((bf16[4,512,512]{1,2,0:T(8,128)(2,1)}), bf16[4,512,512]{1,2,0:T(8,128)(2,1)S(1)}, u32[]{:S(2)}, u32[]{:S(2)}) %all-to-all-start) | async-done | bytes 2097184 | tf_op jit(solution)/shard_map/all_to_all | solution.py:13
  50.7 10.6 %all-gather.9.cloned.1.call-done = bf16[2048,512]{1,0:T(8,128)(2,1)} async-done(((bf16[256,512]{1,0:T(8,128)(2,1)}), bf16[2048,512]{1,0:T(8,128)(2,1)}) %all-gather.9.cloned.1.call-update) | async-done | bytes 2097168 | tf_op jit(solution)/shard_map/all_gather | solution.py:85
  61.3 2.9 fusion.28
  65.2 1.3 copy.34
  67.0 1.4 copy.35
  68.4 2.8 multiply_exponential_fusion
  71.2 2.1 slice.271
  73.3 2.1 slice.272
  75.3 2.1 slice.270
  77.4 2.1 slice.274
  79.5 1.7 fusion.78
  81.2 1.4 slice.277
  82.6 1.4 slice.278
  84.0 1.4 slice.276
  85.3 1.4 slice.280
  86.7 2.0 fusion.79
  90.1 1.6 slice.282
  91.7 1.6 slice.286
  93.3 1.8 fusion.80
  96.3 1.5 slice.288
  97.9 1.5 slice.292
  99.4 1.6 fusion.81
  101.0 1.4 slice.295
  102.5 1.4 slice.296
  103.9 1.5 slice.294
  105.4 1.4 slice.298
  106.8 1.4 fusion.82
  108.2 1.4 slice.301
  109.6 1.4 slice.302
  111.0 1.4 slice.300
  112.3 1.4 slice.304
  113.7 1.4 fusion.83
  116.3 1.3 slice.306
  117.6 1.3 slice.310
  118.9 1.4 fusion.85
  125.5 1.3 slice.305
  128.7 1.4 slice.324
  131.4 1.4 slice.293
  132.8 1.4 slice.326
  135.6 1.5 slice.287
  140.9 1.4 slice.275
  142.3 1.4 slice.332
  152.4 2.7 pad.84
  155.6 6.1 %all-gather.7.cloned.1.call-done = bf16[2048,512]{1,0:T(8,128)(2,1)} async-done(((bf16[256,512]{1,0:T(8,128)(2,1)}), bf16[2048,512]{1,0:T(8,128)(2,1)}) %all-gather.7.cloned.1.call-update) | async-done | bytes 2097168 | tf_op jit(solution)/shard_map/all_gather | solution.py:84
  161.7 7.1 %convolution_convert_fusion.2 = bf16[512,2048]{1,0:T(8,128)(2,1)} fusion(bf16[512,2048]{1,0:T(8,128)(2,1)} %all-gather.11.cloned.1.call-done, bf16[512,2048]{0,1:T(8,128)(2,1)} %bitcast.35, bf16[2048,512]{1,0:T(8,128)(2,1)} %all-gather.7.cloned.1.call-done, f32[512,512]{1,0:T(8,128)S(1)} %pad.83, f32[512,512]{1,0:T(8,128)} %pad.84), kind=kOutput, calls=%fused_computation.5 | convolution fusion | flops 2151940096 | bytes 10485760 | tf_op jit(solution)/shard_map/dot_general | solution.py:105
  170.8 27.9 %reduce-scatter.3.cloned.1.call-done = bf16[512,512]{1,0:T(8,128)(2,1)} async-done(((bf16[512,2048]{1,0:T(8,128)(2,1)}), bf16[512,512]{1,0:T(8,128)(2,1)}) %reduce-scatter.3.cloned.1.call-update) | async-done | bytes 524304 | tf_op jit(solution)/shard_map/reduce_scatter | solution.py:33
  199.9 5.9 %psum.29 = f32[512]{0:T(512)S(1)} all-reduce(f32[512]{0:T(512)S(1)} %fusion.29), channel_id=1, replica_groups=mesh['fs'=8,'tp'=4] {'tp'}, use_global_device_ids=true, to_apply=%region_4.5 | all-reduce | flops 512 | bytes 4096 | tf_op jit(solution)/shard_map/psum | solution.py:23
  205.9 1.5 fusion.37
  207.4 5.7 %psum.30 = f32[512]{0:T(512)S(1)} all-reduce(f32[512]{0:T(512)S(1)} %get-tuple-element.11), channel_id=1, replica_groups=mesh['fs'=8,'tp'=4] {'tp'}, use_global_device_ids=true, to_apply=%region_6.7 | all-reduce | flops 512 | bytes 4096 | tf_op jit(solution)/shard_map/psum | solution.py:23
  213.5 1.5 stack.5
  215.0 3.6 all-to-all-start.1
  218.8 25.4 %all-to-all-done.1 = bf16[4,512,512]{1,2,0:T(8,128)(2,1)S(1)} async-done(((bf16[4,512,512]{1,2,0:T(8,128)(2,1)}), bf16[4,512,512]{1,2,0:T(8,128)(2,1)S(1)}, u32[]{:S(2)}, u32[]{:S(2)}) %all-to-all-start.1) | async-done | bytes 2097184 | tf_op jit(solution)/shard_map/all_to_all | solution.py:13
  244.2 48.9 %all-gather.15.cloned.1.call-done = bf16[2048,1408]{1,0:T(8,128)(2,1)} async-done(((bf16[256,1408]{1,0:T(8,128)(2,1)}), bf16[2048,1408]{1,0:T(8,128)(2,1)}) %all-gather.15.cloned.1.call-update) | async-done | bytes 5767184 | tf_op jit(solution)/shard_map/all_gather | solution.py:118
  293.1 7.7 %fusion = f32[512,1408]{1,0:T(8,128)} fusion(bf16[512,2048]{0,1:T(8,128)(2,1)S(1)} %bitcast.36, bf16[2048,1408]{1,0:T(8,128)(2,1)} %all-gather.15.cloned.1.call-done), kind=kOutput, calls=%fused_computation.2 | convolution fusion | flops 2954231808 | bytes 10747904 | tf_op jit(solution)/shard_map/dot_general | solution.py:52
  300.7 84.9 %all-gather.13.cloned.1.call-done = bf16[2048,1408]{1,0:T(8,128)(2,1)} async-done(((bf16[256,1408]{1,0:T(8,128)(2,1)}), bf16[2048,1408]{1,0:T(8,128)(2,1)}) %all-gather.13.cloned.1.call-update) | async-done | bytes 5767184 | tf_op jit(solution)/shard_map/all_gather | solution.py:117
  385.6 7.7 %fusion.1 = f32[512,1408]{1,0:T(8,128)} fusion(bf16[512,2048]{0,1:T(8,128)(2,1)S(1)} %bitcast.37, bf16[2048,1408]{1,0:T(8,128)(2,1)} %all-gather.13.cloned.1.call-done), kind=kOutput, calls=%fused_computation.4 | convolution fusion | flops 2954231808 | bytes 10747904 | tf_op jit(solution)/shard_map/dot_general | solution.py:51
  393.4 85.6 %all-gather.17.cloned.1.call-done = bf16[1408,2048]{1,0:T(8,128)(2,1)} async-done(((bf16[1408,256]{1,0:T(8,128)(2,1)}), bf16[1408,2048]{1,0:T(8,128)(2,1)}) %all-gather.17.cloned.1.call-update) | async-done | bytes 5767184 | tf_op jit(solution)/shard_map/all_gather | solution.py:126
  479.0 14.7 %convolution_convert_fusion.3 = bf16[512,2048]{1,0:T(8,128)(2,1)} fusion(bf16[1408,2048]{1,0:T(8,128)(2,1)} %all-gather.17.cloned.1.call-done, f32[512,1408]{1,0:T(8,128)} %fusion, f32[512,1408]{1,0:T(8,128)} %fusion.1, f32[1408]{0:T(1024)S(1)} %get-tuple-element.9, f32[1408]{0:T(1024)S(1)} %get-tuple-element.10, f32[1408]{0:T(1024)S(1)} %get-tuple-element.8, ...), kind=kOutput, calls=%fused_computation.6 | convolution fusion | flops 2968256512 | bytes 13665280 | tf_op jit(solution)/shard_map/dot_general | solution.py:124
  493.8 29.5 %reduce-scatter.5.cloned.1.call-done = bf16[512,512]{1,0:T(8,128)(2,1)} async-done(((bf16[512,2048]{1,0:T(8,128)(2,1)}), bf16[512,512]{1,0:T(8,128)(2,1)}) %reduce-scatter.5.cloned.1.call-update) | async-done | bytes 524304 | tf_op jit(solution)/shard_map/reduce_scatter | solution.py:33
  524.5 5.8 %psum.31 = f32[512]{0:T(512)S(1)} all-reduce(f32[512]{0:T(512)S(1)} %fusion.31), channel_id=1, replica_groups=mesh['fs'=8,'tp'=4] {'tp'}, use_global_device_ids=true, to_apply=%region_9.10 | all-reduce | flops 512 | bytes 4096 | tf_op jit(solution)/shard_map/psum | solution.py:23
  530.2 2.1 fusion.40
  (161 shorter events, 38.1 us)
Async XLA Ops:
  6.5 58.1 %copy-start = (bf16[2,256,256]{2,1,0:T(8,128)(2,1)S(1)}, bf16[2,256,256]{2,1,0:T(8,128)(2,1)}, u32[]{:S(2)}) copy-start(bf16[2,256,256]{2,1,0:T(8,128)(2,1)} %param.22) | copy-start | bytes 786436
  6.5 54.8 %all-gather.9.cloned.1.call-start = ((), (), s32[]{:S(2)}) async-start(), calls=%async_computation.5 | async-start | bytes 2359296 | tf_op jit(solution)/shard_map/all_gather | solution.py:85
  7.3 148.3 %all-gather.11.cloned.1.call-start = ((), (), s32[]{:S(2)}) async-start(), calls=%async_computation.6 | async-start | bytes 2359296 | tf_op jit(solution)/shard_map/all_gather | solution.py:107
  21.3 4.5 copy-start.23
  21.3 4.6 copy-start.13
  21.3 29.4 %all-to-all-start = ((bf16[4,512,512]{1,2,0:T(8,128)(2,1)}), bf16[4,512,512]{1,2,0:T(8,128)(2,1)S(1)}, u32[]{:S(2)}, u32[]{:S(2)}) async-start(bf16[4,512,512]{1,2,0:T(8,128)(2,1)} %stack.4), calls=%async_computation | async-start | bytes 4194304 | tf_op jit(solution)/shard_map/all_to_all | solution.py:13
  25.1 136.6 %all-gather.7.cloned.1.call-start = ((), (), s32[]{:S(2)}) async-start(), calls=%async_computation.4 | async-start | bytes 2359296 | tf_op jit(solution)/shard_map/all_gather | solution.py:84
  25.8 172.9 %reduce-scatter.3.cloned.1.call-start = ((), (), s32[]{:S(2)}) async-start(), calls=%async_computation.7 | async-start | bytes 2621440 | tf_op jit(solution)/shard_map/reduce_scatter | solution.py:33
  50.7 13.5 %copy-start.3 = (bf16[4,512,512]{1,2,0:T(8,128)(2,1)}, bf16[4,512,512]{1,2,0:T(8,128)(2,1)S(1)}, u32[]{:S(2)}) copy-start(bf16[4,512,512]{1,2,0:T(8,128)(2,1)S(1)} %all-to-all-done) | copy-start | bytes 6291460
  64.7 1.8 copy-start.27
  140.8 5.2 copy-start.12
  140.8 5.2 copy-start.14
  140.8 5.2 copy-start.15
  140.8 5.2 copy-start.18
  140.8 5.2 copy-start.9
  140.8 6.0 %copy-start.10 = (f32[3,512]{1,0:T(4,128)S(1)}, f32[3,512]{1,0:T(4,128)}, u32[]{:S(2)}) copy-start(f32[3,512]{1,0:T(4,128)} %slice.305) | copy-start | bytes 18436
  140.8 6.0 %copy-start.11 = (f32[3,512]{1,0:T(4,128)S(1)}, f32[3,512]{1,0:T(4,128)}, u32[]{:S(2)}) copy-start(f32[3,512]{1,0:T(4,128)} %slice.322) | copy-start | bytes 18436
  140.8 6.1 %copy-start.22 = (f32[1,512]{1,0:T(1,128)S(1)}, f32[1,512]{1,0:T(1,128)}, u32[]{:S(2)}) copy-start(f32[1,512]{1,0:T(1,128)} %slice.355) | copy-start | bytes 6148
  140.8 6.1 %copy-start.8 = (f32[7,512]{1,0:T(8,128)S(1)}, f32[7,512]{1,0:T(8,128)}, u32[]{:S(2)}) copy-start(f32[7,512]{1,0:T(8,128)} %slice.324) | copy-start | bytes 43012
  140.8 6.1 %copy-start.21 = (f32[1,512]{1,0:T(1,128)S(1)}, f32[1,512]{1,0:T(1,128)}, u32[]{:S(2)}) copy-start(f32[1,512]{1,0:T(1,128)} %slice.354) | copy-start | bytes 6148
  140.9 6.2 %copy-start.7 = (f32[15,512]{1,0:T(8,128)S(1)}, f32[15,512]{1,0:T(8,128)}, u32[]{:S(2)}) copy-start(f32[15,512]{1,0:T(8,128)} %slice.293) | copy-start | bytes 92164
  140.9 7.7 %copy-start.6 = (f32[31,512]{1,0:T(8,128)S(1)}, f32[31,512]{1,0:T(8,128)}, u32[]{:S(2)}) copy-start(f32[31,512]{1,0:T(8,128)} %slice.287) | copy-start | bytes 190468
  145.4 6.6 %copy-start.4 = (f32[127,512]{1,0:T(8,128)S(1)}, f32[127,512]{1,0:T(8,128)}, u32[]{:S(2)}) copy-start(f32[127,512]{1,0:T(8,128)} %slice.275) | copy-start | bytes 780292
  145.4 6.6 %copy-start.5 = (f32[127,512]{1,0:T(8,128)S(1)}, f32[127,512]{1,0:T(8,128)}, u32[]{:S(2)}) copy-start(f32[127,512]{1,0:T(8,128)} %slice.332) | copy-start | bytes 780292
  147.0 5.1 copy-start.20
  152.3 3.0 copy-start.19
  168.8 1.9 copy-start.24
  168.8 2.0 copy-start.25
  168.8 37.1 %copy-start.2 = (bf16[512,512]{1,0:T(8,128)(2,1)S(1)}, bf16[512,512]{1,0:T(8,128)(2,1)}, u32[]{:S(2)}) copy-start(bf16[512,512]{1,0:T(8,128)(2,1)} %param.17) | copy-start | bytes 1572868
  168.8 124.2 %all-gather.15.cloned.1.call-start = ((), (), s32[]{:S(2)}) async-start(), calls=%async_computation.9 | async-start | bytes 6488064 | tf_op jit(solution)/shard_map/all_gather | solution.py:118
  169.4 216.2 %all-gather.13.cloned.1.call-start = ((), (), s32[]{:S(2)}) async-start(), calls=%async_computation.8 | async-start | bytes 6488064 | tf_op jit(solution)/shard_map/all_gather | solution.py:117
  170.0 309.0 %all-gather.17.cloned.1.call-start = ((), (), s32[]{:S(2)}) async-start(), calls=%async_computation.10 | async-start | bytes 6488064 | tf_op jit(solution)/shard_map/all_gather | solution.py:126
  213.4 5.2 copy-start.16
  213.5 5.2 copy-start.17
  215.0 29.2 %all-to-all-start.1 = ((bf16[4,512,512]{1,2,0:T(8,128)(2,1)}), bf16[4,512,512]{1,2,0:T(8,128)(2,1)S(1)}, u32[]{:S(2)}, u32[]{:S(2)}) async-start(bf16[4,512,512]{1,2,0:T(8,128)(2,1)} %stack.5), calls=%async_computation.2 | async-start | bytes 4194304 | tf_op jit(solution)/shard_map/all_to_all | solution.py:13
  218.6 304.7 %reduce-scatter.5.cloned.1.call-start = ((), (), s32[]{:S(2)}) async-start(), calls=%async_computation.11 | async-start | bytes 2621440 | tf_op jit(solution)/shard_map/reduce_scatter | solution.py:33
  479.0 14.7 %copy-start.26 = (bf16[512]{0:T(512)(128)(2,1)S(1)}, bf16[512]{0:T(512)(128)(2,1)}, u32[]{:S(2)}) copy-start(bf16[512]{0:T(512)(128)(2,1)} %param.33) | copy-start | bytes 3076
  479.0 53.3 %copy-start.1 = (bf16[2,256,256]{2,1,0:T(8,128)(2,1)S(1)}, bf16[2,256,256]{2,1,0:T(8,128)(2,1)}, u32[]{:S(2)}) copy-start(bf16[2,256,256]{2,1,0:T(8,128)(2,1)} %param.22) | copy-start | bytes 786436
Sparse Core Ops, SparseCore 0:
  9.5 51.7 all-gather.8
  63.3 48.8 all-gather.10
  114.4 47.2 all-gather.6
  169.0 29.7 reduce-scatter.2
  200.7 92.2 all-gather.14
  295.1 90.4 all-gather.12
  387.7 91.2 all-gather.16
  493.9 29.3 reduce-scatter.4
